TPU v7x, 32 devices: a whole 2x2x4 slice. The times are simulated.
32 devices in a mesh: grp: 2 (over x), ep: 16 (over z, y, core).
Axes of the slice: x: 2, y: 2, z: 4, core: 2. Of those that a mesh axis runs over, the one named last changes fastest.
Arguments:
- hidden_in: bfloat16 [512, 2048], P(('grp', 'ep')), parts along dimension 0, may hold values from -6 to 6
- state_in: float32 [512, 64, 1024], P(('grp', 'ep')), parts along dimension 0, may hold values from -3 to 3
- norm_gain: float32 [2048], replicated, may hold values from 0.1 to 1.9
- w_recept: bfloat16 [2048, 1024], P(None, 'ep'), may hold values from -0.125 to 0.125
- w_key: bfloat16 [2048, 1024], P(None, 'ep'), may hold values from -0.125 to 0.125
- w_value: bfloat16 [2048, 1024], P(None, 'ep'), may hold values from -0.125 to 0.125
- decay_base: float32 [1024], replicated, may hold values from -4 to 2
- w_decay_down: bfloat16 [2048, 128], replicated, may hold values from -0.125 to 0.125
- w_decay_up: bfloat16 [128, 1024], replicated, may hold values from -0.5 to 0.5
- w_remove_down: bfloat16 [2048, 128], replicated, may hold values from -0.125 to 0.125
- w_remove_up: bfloat16 [128, 1024], replicated, may hold values from -1 to 1
- group_gain: float32 [1024], replicated, may hold values from 0.1 to 1.9
- w_out: bfloat16 [1024, 2048], replicated, may hold values from -0.1875 to 0.1875
- ffn_gain: float32 [2048], replicated, may hold values from 0.1 to 1.9
- routes: int32 [512, 2], P(('grp', 'ep')), parts along dimension 0, may hold values from 0 to 3, all different within a row; in each aligned block of 16 rows (0 to 15, 16 to 31, ...) at most 16 rows name the same one
- route_gate: float32 [512, 2], P(('grp', 'ep')), parts along dimension 0, may hold values from 0.1 to 1
- w_gate: bfloat16 [2048, 11264], P(None, 'ep'), may hold values from -0.125 to 0.125
- w_up: bfloat16 [2048, 11264], P(None, 'ep'), may hold values from -0.125 to 0.125
- w_down: bfloat16 [11264, 2048], P('ep'), may hold values from -0.109375 to 0.109375
Outputs:
- mixed_out: bfloat16 [512, 2048], P(('grp', 'ep')), parts along dimension 0
- state_out: float32 [512, 64, 1024], P(('grp', 'ep')), parts along dimension 0
There are 2 independent parts, one for each index of `grp`. A program takes and returns all parts, laid end to end along the dimension named above; an argument that names none is the same for every part. Nothing has to cross between parts.
Inputs may be any that keep to these rules, and one draw needn't show every extreme that they name: `routes`: each row names 2 different experts; in each aligned block of 16 rows (the rows of one device) no expert is named more than 16 times.
All inputs are finite; a program needn't handle non-finite values.
Results may differ from a plain program's by a relative error of at most 0.015.
Values may be sent and summed in bfloat16 or wider, within the bound.
A program may use at most 128 MiB of HBM per device.

v0:
```python
import jax
import jax.numpy as jnp
from jax import lax
from jax.sharding import PartitionSpec as P

EXP_SPLIT = 4


norm_eps = 1e-06
group_eps = 0.00064


def scaled_rows(values, scale_gain):
    floats = values.astype(jnp.float32)
    return (
        floats
        * lax.rsqrt(jnp.mean(floats * floats, axis=-1, keepdims=True) + norm_eps)
        * scale_gain
    )


def update_state(state_in, receptance, new_keys, new_values, decay_rate, removal):
    seq_count = state_in.shape[0]
    head_size = state_in.shape[1]
    head_count = state_in.shape[2] // head_size
    shape_heads = (seq_count, head_count, head_size)
    recept_heads = receptance.astype(jnp.float32).reshape(shape_heads)
    key_heads = new_keys.astype(jnp.float32).reshape(shape_heads)
    value_heads = new_values.astype(jnp.float32).reshape(shape_heads)
    unit_keys = key_heads * lax.rsqrt(
        jnp.sum(key_heads * key_heads, axis=-1, keepdims=True) + norm_eps
    )
    blocks = state_in.reshape(seq_count, head_size, head_count, head_size)
    recalled = jnp.einsum("svhk,shk->svh", blocks, unit_keys, precision=lax.Precision.HIGHEST)
    removed = unit_keys * removal.reshape(shape_heads)
    updated = (
        blocks * decay_rate.reshape(seq_count, 1, head_count, head_size)
        - recalled[..., None] * removed[:, None]
        + jnp.swapaxes(value_heads, 1, 2)[..., None] * key_heads[:, None]
    )
    readout = jnp.einsum("svhk,shk->shv", updated, recept_heads, precision=lax.Precision.HIGHEST)
    return (updated.reshape(state_in.shape), readout)


def group_scale(readout, scale_gain):
    center = readout - jnp.mean(readout, axis=-1, keepdims=True)
    spread = jnp.mean(center * center, axis=-1, keepdims=True)
    normed = center * lax.rsqrt(spread + group_eps)
    return (normed.reshape(readout.shape[0], -1) * scale_gain).astype(jnp.bfloat16)


def decay_of(normed, w_decay_down, w_decay_up, decay_base):
    decay_low = jnp.dot(normed, w_decay_down, preferred_element_type=jnp.float32).astype(
        jnp.bfloat16
    )
    decay_act = jnp.tanh(decay_low.astype(jnp.float32)).astype(jnp.bfloat16)
    decay_pre = decay_base + jnp.dot(decay_act, w_decay_up, preferred_element_type=jnp.float32)
    return jnp.exp(-jnp.exp(-jax.nn.softplus(-decay_pre) - 0.5))


def removal_of(normed, w_remove_down, w_remove_up):
    remove_low = jnp.dot(normed, w_remove_down, preferred_element_type=jnp.float32).astype(
        jnp.bfloat16
    )
    return jax.nn.sigmoid(jnp.dot(remove_low, w_remove_up, preferred_element_type=jnp.float32))


def shards(
    hidden_in,
    state_in,
    norm_gain,
    w_recept,
    w_key,
    w_value,
    decay_base,
    w_decay_down,
    w_decay_up,
    w_remove_down,
    w_remove_up,
    group_gain,
    w_out,
    ffn_gain,
    routes,
    route_gate,
    w_gate,
    w_up,
    w_down,
):
    normed = scaled_rows(hidden_in, norm_gain).astype(jnp.bfloat16)
    shard_rows = lax.all_gather(normed, "ep", axis=0, tiled=True)
    spread = jnp.stack(
        [
            jnp.dot(shard_rows, matrix, preferred_element_type=jnp.float32).astype(jnp.bfloat16)
            for matrix in (w_recept, w_key, w_value)
        ]
    )
    joined = lax.all_to_all(spread, "ep", split_axis=1, concat_axis=2, tiled=True)
    receptance, new_keys, new_values = (joined[0], joined[1], joined[2])
    decay_rate = decay_of(normed, w_decay_down, w_decay_up, decay_base)
    removal = removal_of(normed, w_remove_down, w_remove_up)
    state_out, readout = update_state(
        state_in, receptance, new_keys, new_values, decay_rate, removal
    )
    grouped = group_scale(readout, group_gain)
    residual = hidden_in.astype(jnp.float32) + jnp.dot(
        grouped, w_out, preferred_element_type=jnp.float32
    )
    expert_in = scaled_rows(residual, ffn_gain).astype(jnp.bfloat16)
    ep_size = lax.axis_size("ep")
    experts = ep_size // EXP_SPLIT
    seq_count, model_width = expert_in.shape
    top_count = routes.shape[1]
    capacity = max(2, 2 * seq_count * top_count // experts)
    chosen = routes.reshape(-1)
    hit_table = (chosen[:, None] == jnp.arange(experts, dtype=jnp.int32)[None, :]).astype(jnp.int32)
    slot_index = jnp.sum((jnp.cumsum(hit_table, axis=0) - 1) * hit_table, axis=1)
    slot_table = (slot_index[:, None] == jnp.arange(capacity, dtype=jnp.int32)[None, :]).astype(
        jnp.float32
    )
    placed = hit_table.astype(jnp.float32)[:, :, None] * slot_table[:, None, :]
    placed = placed.reshape(seq_count, top_count, experts * capacity)
    dispatch = jnp.sum(placed, axis=1).astype(jnp.bfloat16)
    combine = jnp.sum(placed * route_gate[:, :, None], axis=1)
    outgoing = jnp.einsum(
        "sm,sd->md", dispatch, expert_in, preferred_element_type=jnp.float32
    ).astype(jnp.bfloat16)
    send_buffer = jnp.broadcast_to(
        outgoing.reshape(experts, 1, capacity, model_width),
        (experts, EXP_SPLIT, capacity, model_width),
    )
    send_buffer = send_buffer.reshape(ep_size, capacity, model_width)
    columns = lax.all_to_all(send_buffer, "ep", split_axis=0, concat_axis=0, tiled=True)
    flat_rows = columns.reshape(-1, model_width)
    gate_pre = jnp.dot(flat_rows, w_gate, preferred_element_type=jnp.float32)
    up_pre = jnp.dot(flat_rows, w_up, preferred_element_type=jnp.float32)
    hidden = (jax.nn.silu(gate_pre) * up_pre).astype(jnp.bfloat16)
    partial_out = jnp.dot(hidden, w_down, preferred_element_type=jnp.float32).astype(jnp.bfloat16)
    partial_out = partial_out.reshape(columns.shape[0], columns.shape[1], model_width)
    returned = lax.all_to_all(partial_out, "ep", split_axis=0, concat_axis=0, tiled=True)
    summed = jnp.sum(
        returned.reshape(experts, EXP_SPLIT, capacity, model_width).astype(jnp.float32), axis=1
    )
    routed = jnp.dot(
        combine, summed.reshape(experts * capacity, model_width), precision=lax.Precision.HIGHEST
    )
    mixed_out = (residual + routed).astype(jnp.bfloat16)
    return (mixed_out, state_out)


def solution(mesh):
    placed = (
        P(("grp", "ep"), None),
        P(("grp", "ep"), None, None),
        P(),
        P(None, "ep"),
        P(None, "ep"),
        P(None, "ep"),
        P(),
        P(),
        P(),
        P(),
        P(),
        P(),
        P(),
        P(),
        P(("grp", "ep"), None),
        P(("grp", "ep"), None),
        P(None, "ep"),
        P(None, "ep"),
        P("ep", None),
    )
    return jax.shard_map(
        shards,
        mesh=mesh,
        in_specs=placed,
        out_specs=(P(("grp", "ep"), None), P(("grp", "ep"), None, None)),
        check_vma=False,
    )
```

profile of v0, /device:TPU:0, one launch (start us, length us, event | category | flops | bytes accessed | tf_op | source)
XLA Modules:
  0.0 197.7 jit_solution(5547005113535397011)
XLA Ops:
  7.2 1.1 fusion.15
  8.4 1.6 fusion.17
  9.9 0.8 copy.54
  10.9 0.2 select_reduce_fusion
  11.2 1.5 fusion.23
  12.7 38.6 %all-gather.2.cloned.1.call-done = bf16[256,2048]{1,0:T(8,128)(2,1)} async-done(((bf16[16,2048]{1,0:T(8,128)(2,1)}), bf16[256,2048]{1,0:T(8,128)(2,1)}) %all-gather.2.cloned.1.call-update) | async-done | bytes 1048592 | tf_op jit(solution)/shard_map/all_gather | solution.py:90
  51.4 1.7 fusion.10
  53.1 1.7 fusion.9
  54.8 1.7 fusion.8
  56.5 0.2 copy.48
  56.7 0.8 reshape.183
  57.5 3.7 %all-to-all-start = ((bf16[16,2,1536]{2,1,0:T(2,128)(2,1)}), bf16[16,2,1536]{2,1,0:T(2,128)(2,1)S(1)}, u32[]{:S(2)}, u32[]{:S(2)}) async-start(bf16[16,2,1536]{2,1,0:T(2,128)(2,1)} %reshape.183), calls=%async_computation | async-start | bytes 196608 | tf_op jit(solution)/shard_map/all_to_all | solution.py:97
  61.6 7.3 %reshape.167 = f32[16,64,16,64]{3,2,1,0:T(8,128)} reshape(f32[16,64,1024]{2,1,0:T(8,128)} %param.20) | data formatting | bytes 8388608 | tf_op jit(solution)/shard_map/reshape | solution.py:33
  68.9 0.6 fusion.33
  69.5 0.2 reshape.184
  69.9 0.7 slice_convert_fusion
  70.7 0.7 mul.186.clone
  71.4 1.0 mul.217
  72.4 1.6 copy.56
  74.0 1.0 reshape.177
  75.0 2.1 %multiply_multiply_fusion = (f32[16,1024]{1,0:T(8,128)}, f32[16,1024]{1,0:T(8,128)}) fusion(f32[16,1024]{1,0:T(8,128)S(1)} %reshape.177, f32[16,1024]{1,0:T(8,128)S(1)} %mul.217, bf16[128,1024]{1,0:T(8,128)(2,1)} %param.29, bf16[16,2048]{1,0:T(8,128)(2,1)S(1)} %copy-done.4, bf16[2048,128]{1,0:T(8,128)(2,1)} %param.28), kind=kOutput, calls=%fused_computation.54 | convolution fusion | flops 12666880 | bytes 1114112 | tf_op jit(solution)/shard_map/dot_general | solution.py:65
  77.1 1.6 reshape.168
  78.7 1.0 broadcast_multiply_fusion
  79.7 0.7 copy.67
  80.4 0.7 copy.51
  81.1 0.7 copy.53
  81.8 1.1 copy.52
  83.0 5.8 %multiply_reduce_fusion = f32[16,16,64]{1,2,0:T(8,128)S(1)} fusion(f32[16,64,16,64]{3,2,1,0:T(8,128)} %reshape.167, f32[16,16,64]{2,1,0:T(8,128)} %copy.67), kind=kLoop, calls=%fused_computation.2 | loop fusion | flops 2080768 | bytes 4325376 | tf_op jit(solution)/shard_map/svhk,shk->svh/dot_general | solution.py:34
  88.8 5.1 %multiply_add_fusion = f32[16,64,16,64]{3,2,1,0:T(8,128)S(1)} fusion(f32[16,64,16,64]{3,2,1,0:T(8,128)S(1)} %copy-done.2, f32[16,16,64]{2,1,0:T(8,128)S(1)} %copy-done.12, f32[16,64,16]{2,1,0:T(8,128)S(1)} %copy.52, f32[16,16,64]{2,1,0:T(8,128)S(1)} %copy-done.11, f32[16,64,16]{2,1,0:T(8,128)S(1)} %bitcast.69, f32[16,16,64]{2,1,0:T(8,128)S(1)} %mul.182), kind=kLoop, calls=%fused_computation.3 | loop fusion | flops 5242880 | bytes 8716288 | tf_op jit(solution)/shard_map/add | solution.py:37
  94.0 8.5 %fusion = f32[16,16,1,64]{3,2,1,0:T(1,128)S(1)} fusion(f32[16,64,16,64]{3,2,1,0:T(8,128)S(1)} %multiply_add_fusion, bf16[16,16,64,1]{2,0,1,3:T(8,128)(2,1)S(1)} %copy-done.6), kind=kOutput, calls=%fused_computation | convolution fusion | flops 12582912 | bytes 4292608 | tf_op jit(solution)/shard_map/svhk,shk->shv/dot_general | solution.py:41
  102.5 0.1 reduce_sum.83
  102.6 0.2 multiply_reduce_fusion.2
  102.8 0.8 subtract_multiply_fusion
  103.6 1.6 reshape.170
  105.2 3.2 %multiply_reduce_fusion.1 = (f32[16]{0:T(128)S(1)}, f32[16,2048]{1,0:T(8,128)S(1)}) fusion(bf16[1024,2048]{1,0:T(8,128)(2,1)} %param.31, f32[16,1024]{1,0:T(8,128)} %reshape.170, f32[1024]{0:T(1024)} %param.30, bf16[16,2048]{1,0:T(8,128)(2,1)} %param.19), kind=kOutput, calls=%fused_computation.41 | convolution fusion | flops 67272688 | bytes 4460608 | tf_op jit(solution)/shard_map/dot_general | solution.py:105
  108.4 0.3 convolution_convert_fusion.1
  108.8 30.5 %all_to_all.25 = bf16[16,16,2048]{2,1,0:T(8,128)(2,1)S(1)} all-to-all(bf16[16,16,2048]{2,1,0:T(8,128)(2,1)S(1)} %bitcast.71), channel_id=1, replica_groups=mesh['grp'=2,'ep'=16] {'ep'}, dimensions={0} | all-to-all | bytes 2097152 | tf_op jit(solution)/shard_map/all_to_all | solution.py:132
  139.3 1.0 copy-done.5
  140.3 1.8 fusion.34
  142.1 6.6 %convolution_convert_fusion = bf16[256,2048]{1,0:T(8,128)(2,1)} fusion(bf16[704,2048]{1,0:T(8,128)(2,1)S(1)} %copy-done, bf16[256,2048]{1,0:T(8,128)(2,1)} %bitcast.83, bf16[2048,704]{0,1:T(8,128)(2,1)} %param.36, f32[256,704]{0,1:T(8,128)} %fusion.34), kind=kOutput, calls=%fused_computation.5 | convolution fusion | flops 1478000640 | bytes 8585216 | tf_op jit(solution)/shard_map/dot_general | solution.py:137
  148.7 5.1 %all-to-all-start.2 = ((bf16[16,16,2048]{2,1,0:T(8,128)(2,1)}), bf16[16,16,2048]{2,1,0:T(8,128)(2,1)}, u32[]{:S(2)}, u32[]{:S(2)}) async-start(bf16[16,16,2048]{2,1,0:T(8,128)(2,1)} %bitcast.81), calls=%async_computation.2 | async-start | bytes 2097152 | tf_op jit(solution)/shard_map/all_to_all | solution.py:139
  153.8 5.8 %mul.188 = f32[16,64,16,64]{3,2,1,0:T(8,128)} broadcast(f32[16,64,16]{2,1,0:T(8,128)} %bitcast.70), dimensions={0,1,2} | broadcast | bytes 4259840 | tf_op jit(solution)/shard_map/mul | solution.py:38
  159.7 7.6 %mul.216 = f32[16,64,1024]{2,1,0:T(8,128)} reshape(f32[16,64,16,64]{3,2,1,0:T(8,128)} %mul.188) | data formatting | bytes 8388608 | tf_op jit(solution)/shard_map/mul | solution.py:38
  167.3 4.5 %mul.192 = f32[16,64,16,64]{3,2,1,0:T(8,128)} broadcast(f32[16,64,16]{2,1,0:T(8,128)S(1)} %copy.52), dimensions={0,1,2} | broadcast | bytes 4259840 | tf_op jit(solution)/shard_map/mul | solution.py:39
  171.8 7.6 %mul.222 = f32[16,64,1024]{2,1,0:T(8,128)} reshape(f32[16,64,16,64]{3,2,1,0:T(8,128)} %mul.192) | data formatting | bytes 8388608 | tf_op jit(solution)/shard_map/mul | solution.py:39
  179.5 8.9 %multiply_add_fusion.1 = f32[16,64,1024]{2,1,0:T(8,128)} fusion(f32[16,64,1024]{2,1,0:T(8,128)} %mul.222, f32[16,64,1024]{2,1,0:T(8,128)} %mul.216, f32[16,64,1024]{2,1,0:T(8,128)} %param.20, f32[16,1024]{1,0:T(8,128)S(1)} %copy-done.10, f32[16,1024]{1,0:T(8,128)S(1)} %copy-done.13, f32[16,1024]{1,0:T(8,128)S(1)} %copy-done.8), kind=kLoop, calls=%fused_computation.4 | loop fusion | flops 5242880 | bytes 16973824 | tf_op jit(solution)/shard_map/add | solution.py:37
  188.4 1.4 convert_reduce_fusion
  189.8 1.0 fusion.2
  (57 shorter events, 1.2 us)
Async XLA Ops:
  7.2 134.9 %copy-start = (bf16[704,2048]{1,0:T(8,128)(2,1)S(1)}, bf16[704,2048]{1,0:T(8,128)(2,1)}, u32[]{:S(2)}) copy-start(bf16[704,2048]{1,0:T(8,128)(2,1)} %param.37) | copy-start | bytes 8650756
  7.2 54.2 %copy-start.16 = (f32[16,2]{0,1:T(2,128)S(1)}, f32[16,2]{0,1:T(2,128)}, u32[]{:S(2)}) copy-start(f32[16,2]{0,1:T(2,128)} %param.34) | copy-start | bytes 388
  7.2 44.2 %all-gather.2.cloned.1.call-start = ((), (), s32[]{:S(2)}) async-start(), calls=%async_computation.3 | async-start | bytes 1114112 | tf_op jit(solution)/shard_map/all_gather | solution.py:90
  12.7 56.2 %copy-start.7 = (f32[16,1024]{1,0:T(8,128)}, f32[16,1024]{1,0:T(8,128)S(1)}, u32[]{:S(2)}) copy-start(f32[16,1024]{1,0:T(8,128)S(1)} %fusion.23) | copy-start | bytes 196612
  57.5 12.0 %all-to-all-start = ((bf16[16,2,1536]{2,1,0:T(2,128)(2,1)}), bf16[16,2,1536]{2,1,0:T(2,128)(2,1)S(1)}, u32[]{:S(2)}, u32[]{:S(2)}) async-start(bf16[16,2,1536]{2,1,0:T(2,128)(2,1)} %reshape.183), calls=%async_computation | async-start | bytes 196608 | tf_op jit(solution)/shard_map/all_to_all | solution.py:97
  61.6 13.4 %copy-start.4 = (bf16[16,2048]{1,0:T(8,128)(2,1)S(1)}, bf16[16,2048]{1,0:T(8,128)(2,1)}, u32[]{:S(2)}) copy-start(bf16[16,2048]{1,0:T(8,128)(2,1)} %fusion.17) | copy-start | bytes 196612
  75.0 6.8 %copy-start.9 = (f32[16,1024]{1,0:T(8,128)}, f32[16,1024]{1,0:T(8,128)S(1)}, u32[]{:S(2)}) copy-start(f32[16,1024]{1,0:T(8,128)S(1)} %reshape.177) | copy-start | bytes 196612
  82.9 5.8 %copy-start.2 = (f32[16,64,16,64]{3,2,1,0:T(8,128)S(1)}, f32[16,64,16,64]{3,2,1,0:T(8,128)}, u32[]{:S(2)}) copy-start(f32[16,64,16,64]{3,2,1,0:T(8,128)} %reshape.167) | copy-start | bytes 12582916
  82.9 5.8 %copy-start.11 = (f32[16,16,64]{2,1,0:T(8,128)S(1)}, f32[16,16,64]{2,1,0:T(8,128)}, u32[]{:S(2)}) copy-start(f32[16,16,64]{2,1,0:T(8,128)} %copy.51) | copy-start | bytes 196612
  83.0 5.8 %copy-start.12 = (f32[16,16,64]{2,1,0:T(8,128)S(1)}, f32[16,16,64]{2,1,0:T(8,128)}, u32[]{:S(2)}) copy-start(f32[16,16,64]{2,1,0:T(8,128)} %copy.53) | copy-start | bytes 196612
  88.8 5.2 %copy-start.3 = (f32[16,16,64]{1,2,0:T(8,128)}, f32[16,16,64]{1,2,0:T(8,128)S(1)}, u32[]{:S(2)}) copy-start(f32[16,16,64]{1,2,0:T(8,128)S(1)} %multiply_reduce_fusion) | copy-start | bytes 196612
  88.8 5.2 %copy-start.6 = (bf16[16,16,64,1]{2,0,1,3:T(8,128)(2,1)S(1)}, bf16[16,16,64,1]{2,0,1,3:T(8,128)(2,1)}, u32[]{:S(2)}) copy-start(bf16[16,16,64,1]{2,0,1,3:T(8,128)(2,1)} %get-tuple-element.8) | copy-start | bytes 98308
  103.6 4.8 %copy-start.14 = (bf16[16,64]{1,0:T(8,128)(2,1)S(1)}, bf16[16,64]{1,0:T(8,128)(2,1)}, u32[]{:S(2)}) copy-start(bf16[16,64]{1,0:T(8,128)(2,1)} %get-tuple-element.2) | copy-start | bytes 6148
  105.2 3.2 %copy-start.15 = (f32[2048]{0:T(1024)S(1)}, f32[2048]{0:T(1024)}, u32[]{:S(2)}) copy-start(f32[2048]{0:T(1024)} %param.32) | copy-start | bytes 24580
  105.2 35.0 %copy-start.17 = (bf16[2048,704]{0,1:T(8,128)(2,1)S(1)}, bf16[2048,704]{0,1:T(8,128)(2,1)}, u32[]{:S(2)}) copy-start(bf16[2048,704]{0,1:T(8,128)(2,1)} %param.35) | copy-start | bytes 8650756
  139.3 1.0 copy-start.5
  148.7 39.6 %all-to-all-start.2 = ((bf16[16,16,2048]{2,1,0:T(8,128)(2,1)}), bf16[16,16,2048]{2,1,0:T(8,128)(2,1)}, u32[]{:S(2)}, u32[]{:S(2)}) async-start(bf16[16,16,2048]{2,1,0:T(8,128)(2,1)} %bitcast.81), calls=%async_computation.2 | async-start | bytes 2097152 | tf_op jit(solution)/shard_map/all_to_all | solution.py:139
  171.8 7.7 %copy-start.8 = (f32[16,1024]{1,0:T(8,128)S(1)}, f32[16,1024]{1,0:T(8,128)}, u32[]{:S(2)}) copy-start(f32[16,1024]{1,0:T(8,128)} %copy-done.7) | copy-start | bytes 196612
  171.8 7.7 %copy-start.10 = (f32[16,1024]{1,0:T(8,128)S(1)}, f32[16,1024]{1,0:T(8,128)}, u32[]{:S(2)}) copy-start(f32[16,1024]{1,0:T(8,128)} %copy-done.9) | copy-start | bytes 196612
  171.8 7.7 %copy-start.13 = (f32[16,1024]{1,0:T(8,128)S(1)}, f32[16,1024]{1,0:T(8,128)}, u32[]{:S(2)}) copy-start(f32[16,1024]{1,0:T(8,128)} %get-tuple-element.14) | copy-start | bytes 196612
  179.5 11.3 %copy-start.1 = (bf16[704,2048]{1,0:T(8,128)(2,1)S(1)}, bf16[704,2048]{1,0:T(8,128)(2,1)}, u32[]{:S(2)}) copy-start(bf16[704,2048]{1,0:T(8,128)(2,1)} %param.37) | copy-start | bytes 8650756
Sparse Core Ops, SparseCore 0:
  10.7 40.5 all-gather.1
where the time goes:
time: 199 us; the launch traced here: 198 us
  local copies, waits for them, and re-layouts  47.2 us (24%)
  waiting for transfers between devices  38.7 us (19%)
  blocking collectives  30.5 us (15%)
  matrix products  30.2 us (15%)
  other arithmetic  28 us (14%)
  between operations  14.4 us (7%)
  starting transfers between devices  8.8 us (4%)
    all_gather x1, waiting for transfers between devices, shards(): shard_rows = lax.all_gather(normed, 'ep', axis=0, tiled=True)  38.6 us
    all_to_all x1, blocking collectives, shards(): lax.all_to_all(send_buffer, 'ep', split_axis=0, concat_axis=0, tiled=True)  30.5 us
    add x2, other arithmetic, update_state(): blocks * decay_rate.reshape(seq_count, 1, head_count, head_size)  14 us
    mul x2, local copies, waits for them, and re-layouts, update_state(): recalled[..., None] * removed[:, None]  13.5 us
    mul x2, local copies, waits for them, and re-layouts, update_state(): jnp.swapaxes(value_heads, 1, 2)[..., None] * key_heads[:, None]  12.2 us
    dot_general x1, matrix products, update_state(): jnp.einsum('svhk,shk->shv', updated, recept_heads, precision=lax.Precisio...  8.51 us
    reshape x1, local copies, waits for them, and re-layouts, update_state(): blocks = state_in.reshape(seq_count, head_size, head_count, head_size)  7.28 us
    dot_general x1, matrix products, shards(): jnp.dot(hidden, w_down, preferred_element_type=jnp.float32)  6.64 us
  transfers between devices with their start and end apart: 3, of which 1 were waited for; matrix products, arithmetic and copies ran while one was open for 23% of the time, Pallas kernels for 0%

commit v1 on v0

v1 whole, which is shorter than its diff:
```python
import functools

import jax
import jax.numpy as jnp
from jax import lax
from jax.experimental import pallas as pl
from jax.experimental.pallas import tpu as pltpu
from jax.sharding import PartitionSpec as P

EXP_SPLIT = 4
MESH = pl.DeviceIdType.MESH
F32 = jnp.float32
BF16 = jnp.bfloat16

norm_eps = 1e-06
group_eps = 0.00064


def scaled_rows(values, scale_gain):
    floats = values.astype(F32)
    return (
        floats
        * lax.rsqrt(jnp.mean(floats * floats, axis=-1, keepdims=True) + norm_eps)
        * scale_gain
    )


def dot(lhs, rhs):
    return jnp.dot(lhs, rhs, preferred_element_type=F32)


def dot_t(lhs, rhs):
    return lax.dot_general(lhs, rhs, (((1,), (1,)), ((), ())), preferred_element_type=F32)


def split_dot(lhs, rhs):
    high = lhs.astype(BF16)
    low = (lhs - high.astype(F32)).astype(BF16)
    return dot(high, rhs) + dot(low, rhs)


def remote(src, dst, send_sem, recv_sem, device):
    return pltpu.make_async_remote_copy(
        src_ref=src,
        dst_ref=dst,
        send_sem=send_sem,
        recv_sem=recv_sem,
        device_id={"ep": device},
        device_id_type=MESH,
    )


def place(ep_size):
    me = lax.axis_index("ep")
    return me, me // 4, (me // 2) % 2, me % 2, ep_size // 4


def greet_all(me, ep_size):
    barrier = pltpu.get_barrier_semaphore()
    for step in range(1, ep_size):
        pl.semaphore_signal(
            barrier, inc=1, device_id={"ep": lax.rem(me + step, ep_size)}, device_id_type=MESH
        )
    return barrier


class Gather:
    def __init__(self, ep_size, slots, z_sems, b_sems, c_sems):
        self.me, self.a, self.b, self.c, self.planes = place(ep_size)
        self.slots = slots
        self.z, self.bs, self.cs = z_sems, b_sems, c_sems
        self.sent = []

    def slot(self, core, back, side):
        plane = lax.rem(self.a + (self.planes - back), self.planes)
        return self.slots.at[core, plane * 2 + side]

    def device(self, plane, side, core):
        return (plane * 2 + side) * 2 + core

    def along(self, i):
        ref = self.slot(self.c, 0, self.b)
        plane = lax.rem(self.a + i, self.planes)
        return remote(
            ref, ref, self.z.at[0, i], self.z.at[1, i], self.device(plane, self.b, self.c)
        )

    def across(self, i):
        ref = self.slot(self.c, i, self.b)
        return remote(
            ref, ref, self.bs.at[0, i], self.bs.at[1, i], self.device(self.a, 1 - self.b, self.c)
        )

    def to_core(self, kind, i):
        ref = self.slot(self.c, i, self.b if kind == 0 else 1 - self.b)
        return remote(
            ref,
            ref,
            self.cs.at[0, kind, i],
            self.cs.at[1, kind, i],
            self.device(self.a, self.b, 1 - self.c),
        )

    def go(self, copy):
        copy.start()
        self.sent.append(copy)

    def start(self):
        for i in reversed(range(1, self.planes)):
            self.go(self.along(i))
        self.go(self.across(0))
        self.go(self.to_core(0, 0))

    def arrived(self, ref, sem):
        remote(ref, ref, sem, sem, self.me).wait_recv()

    def relay_side(self, i):
        self.arrived(self.slot(self.c, i, 1 - self.b), self.bs.at[1, i])
        self.go(self.to_core(1, i))

    def finish(self):
        for i in range(1, self.planes):
            self.arrived(self.slot(self.c, i, self.b), self.z.at[1, i])
            self.go(self.across(i))
            self.go(self.to_core(0, i))
            self.relay_side(i - 1)
        self.relay_side(self.planes - 1)

    def finish_core(self):
        for i in range(self.planes):
            self.arrived(self.slot(1 - self.c, i, self.b), self.cs.at[1, 0, i])
            self.arrived(self.slot(1 - self.c, i, 1 - self.b), self.cs.at[1, 1, i])

    def drain(self):
        for copy in self.sent:
            copy.wait_send()


def gather_scratch(ep_size, rows, width):
    planes = ep_size // 4
    return [
        pltpu.VMEM((2, ep_size // 2, rows, width), BF16),
        pltpu.SemaphoreType.DMA((2, planes)),
        pltpu.SemaphoreType.DMA((2, planes)),
        pltpu.SemaphoreType.DMA((2, 2, planes)),
    ]


def load_all(pairs, sems):
    copies = [pltpu.make_async_copy(src, dst, sems.at[n]) for n, (src, dst) in enumerate(pairs)]
    for copy in copies:
        copy.start()
    return copies


def project_kernel(
    ep_size, experts, hidden_ref, gain_ref, base_ref, routes_ref, gates_ref,
    wr, wk, wv, wdd, wdu, wrd, wru,
    got_ref, decay_ref, removal_ref,
    wdd_v, wdu_v, wrd_v, wru_v, load_sems,
    joint, slots, z_sems, b_sems, c_sems, outbox, inbox, x_send, x_recv,
):
    me, a, b, c, planes = place(ep_size)
    rows, width = hidden_ref.shape
    part = wr.shape[0]
    lanes = joint.shape[0]
    barrier = greet_all(me, ep_size)
    loads = load_all(
        [(wdd, wdd_v), (wrd, wrd_v), (wdu, wdu_v), (wru, wru_v)]
        + [(w, joint.at[pl.ds(n * part, part)]) for n, w in enumerate((wr, wk, wv))],
        load_sems,
    )
    if lanes > 3 * part:
        joint[3 * part :, :] = jnp.zeros((lanes - 3 * part, joint.shape[1]), BF16)
    normed = scaled_rows(hidden_ref[...], gain_ref[...]).astype(BF16)
    slots[c, a * 2 + b] = normed
    pl.semaphore_wait(barrier, ep_size - 1)
    gather = Gather(ep_size, slots, z_sems, b_sems, c_sems)
    gather.start()

    for copy in loads[:4]:
        copy.wait()
    decay_low = dot(normed, wdd_v[...]).astype(BF16)
    decay_act = jnp.tanh(decay_low.astype(F32)).astype(BF16)
    decay_pre = base_ref[...] + dot(decay_act, wdu_v[...])
    decay_ref[...] = jnp.exp(-jnp.exp(-jax.nn.softplus(-decay_pre) - 0.5))
    remove_low = dot(normed, wrd_v[...]).astype(BF16)
    removal_ref[...] = jax.nn.sigmoid(dot(remove_low, wru_v[...]))
    for copy in loads[4:]:
        copy.wait()
    lane = lax.broadcasted_iota(jnp.int32, (rows, lanes), 1) - 3 * part
    weight = jnp.zeros((rows, lanes), F32)
    for j in range(routes_ref.shape[1]):
        chosen = routes_ref[:, j : j + 1]
        hit = (lane == chosen) | (lane == chosen + experts)
        weight = weight + jnp.where(hit, gates_ref[:, j : j + 1], 0.0)
    high = weight.astype(BF16).astype(F32)
    spare = jnp.where(lane < experts, high, weight - high)
    spare = jnp.where(lane >= 0, spare, 0.0)

    gather.finish()
    gather.finish_core()
    rows_all = slots[...].reshape(ep_size * rows, width)
    spread = dot_t(rows_all, joint[...]).reshape(2, ep_size // 2, rows, lanes)
    outbox[...] = (spread + spare[None, None]).astype(BF16)
    sends = []
    for step in range(1, ep_size):
        other = lax.rem(me + step, ep_size)
        copy = remote(
            outbox.at[other % 2, other // 2],
            inbox.at[c, a * 2 + b],
            x_send.at[step],
            x_recv.at[step],
            other,
        )
        copy.start()
        sends.append(copy)
    inbox[c, a * 2 + b] = outbox[c, a * 2 + b]
    for step in range(1, ep_size):
        other = lax.rem(me + (ep_size - step), ep_size)
        ref = inbox.at[other % 2, other // 2]
        remote(ref, ref, x_recv.at[step], x_recv.at[step], me).wait_recv()
    got_ref[...] = inbox[...]
    gather.drain()
    for copy in sends:
        copy.wait_send()


def mixer_kernel(
    ep_size, hidden_ref, got_ref, decay_ref, removal_ref, ggain_ref, fgain_ref, state_ref, w_out,
    state_out, residual_ref, expert_ref,
    w_out_v, load_sem, recept, keys, values, group, grouped,
):
    step = pl.program_id(0)
    seqs, head, inner = state_ref.shape
    heads = inner // head
    part = inner // ep_size
    load = pltpu.make_async_copy(w_out, w_out_v, load_sem)

    @pl.when(step == 0)
    def _():
        load.start()
        for d in range(ep_size):
            block = got_ref[d % 2, d // 2].astype(F32)
            own = slice(d * part, (d + 1) * part)
            recept[:, own] = block[:, 0:part]
            keys[:, own] = block[:, part : 2 * part]
            values[:, own] = block[:, 2 * part : 3 * part]
        group[...] = (
            lax.broadcasted_iota(jnp.int32, (inner, heads), 0) // head
            == lax.broadcasted_iota(jnp.int32, (inner, heads), 1)
        ).astype(F32).astype(BF16)

    these = pl.ds(pl.multiple_of(step * seqs, seqs), seqs)
    spread = (
        lax.broadcasted_iota(jnp.int32, (heads, inner), 1) // head
        == lax.broadcasted_iota(jnp.int32, (heads, inner), 0)
    ).astype(F32).astype(BF16)
    own_row = (
        lax.broadcasted_iota(jnp.int32, (head, inner), 1) % head
        == lax.broadcasted_iota(jnp.int32, (head, inner), 0)
    ).astype(F32)
    gather = group[...]
    key = keys[these, :]
    sums = split_dot(key * key, gather)
    unit = key * split_dot(lax.rsqrt(sums + norm_eps), spread)
    removed = unit * removal_ref[these, :]
    recept_now = recept[these, :]
    value_now = values[these, :]
    decay = decay_ref[these, :]
    out_rows = []
    for s in range(seqs):
        one = slice(s, s + 1)
        block = state_ref[s]
        recalled = split_dot(block * unit[one], gather)
        value_col = dot((own_row * value_now[one]).astype(BF16), gather)
        updated = (
            block * decay[one]
            - split_dot(recalled, spread) * removed[one]
            + dot(value_col.astype(BF16), spread) * key[one]
        )
        state_out[s] = updated
        readout = split_dot(updated * recept_now[one], gather)
        center = readout - jnp.mean(readout, axis=0, keepdims=True)
        var = jnp.mean(center * center, axis=0, keepdims=True)
        normed = center * lax.rsqrt(var + group_eps)
        out_rows.append(jnp.sum(split_dot(normed, spread) * own_row, axis=0, keepdims=True))
    grouped[these, :] = jnp.concatenate(out_rows, axis=0) * ggain_ref[...]

    @pl.when(step == pl.num_programs(0) - 1)
    def _():
        load.wait()
        residual = hidden_ref[...].astype(F32) + dot(grouped[...].astype(BF16), w_out_v[...])
        residual_ref[...] = residual
        expert_ref[...] = scaled_rows(residual, fgain_ref[...]).astype(BF16)


def expert_kernel(
    ep_size, experts, part, expert_ref, residual_ref, got_ref, wg, wu, wd,
    mixed_ref,
    wg_v, wu_v, wd_v, load_sems,
    slots, z_sems, b_sems, c_sems,
    mine, c_out, c_in, c_sem, b_out, b_in, b_sem, z_out, z_in, z_sem,
):
    me, a, b, c, planes = place(ep_size)
    rows, width = expert_ref.shape
    half = ep_size // 2
    barrier = greet_all(me, ep_size)
    loads = load_all([(wg, wg_v), (wu, wu_v), (wd, wd_v)], load_sems)
    slots[c, a * 2 + b] = expert_ref[...]
    pl.semaphore_wait(barrier, ep_size - 1)
    gather = Gather(ep_size, slots, z_sems, b_sems, c_sems)
    gather.start()
    expert = me // EXP_SPLIT
    lane = lax.broadcasted_iota(jnp.int32, got_ref.shape[2:], 1) - 3 * part
    column = (lane == expert) | (lane == expert + experts)
    for copy in loads:
        copy.wait()

    def run(core):
        flat = slots[core].reshape(half * rows, width)
        gate_pre = dot_t(flat, wg_v[...])
        up_pre = dot_t(flat, wu_v[...])
        hidden = (jax.nn.silu(gate_pre) * up_pre).astype(BF16)
        weight = jnp.sum(
            jnp.where(column[None], got_ref[core].astype(F32), 0.0), axis=-1, keepdims=True
        )
        return dot(hidden, wd_v[...]).reshape(half, rows, width) * weight

    gather.finish()
    gather.finish_core()
    sends = []
    c_out[...] = run(1 - c).astype(BF16)
    for i in range(planes):
        plane = lax.rem(a + i, planes)
        copy = remote(
            c_out.at[pl.ds(plane * 2, 2)],
            c_in.at[pl.ds(plane * 2, 2)],
            c_sem.at[0, i],
            c_sem.at[1, i],
            (a * 2 + b) * 2 + 1 - c,
        )
        copy.start()
        sends.append(copy)
    mine[...] = run(c)
    order = list(range(1, planes)) + [0]
    for i in order:
        plane = lax.rem(a + i, planes)
        both = c_in.at[pl.ds(plane * 2, 2)]
        remote(both, both, c_sem.at[1, i], c_sem.at[1, i], me).wait_recv()
        far = plane * 2 + 1 - b
        b_out[plane] = (mine[far] + c_in[far].astype(F32)).astype(BF16)
        copy = remote(
            b_out.at[plane],
            b_in.at[plane],
            b_sem.at[0, i],
            b_sem.at[1, i],
            (a * 2 + 1 - b) * 2 + c,
        )
        copy.start()
        sends.append(copy)
    total = residual_ref[...]
    for i in order:
        plane = lax.rem(a + i, planes)
        ref = b_in.at[plane]
        remote(ref, ref, b_sem.at[1, i], b_sem.at[1, i], me).wait_recv()
        near = plane * 2 + b
        joined = mine[near] + c_in[near].astype(F32) + b_in[plane].astype(F32)
        if i == 0:
            total = total + joined
        else:
            z_out[i] = joined.astype(BF16)
            copy = remote(
                z_out.at[i],
                z_in.at[i],
                z_sem.at[0, i],
                z_sem.at[1, i],
                (plane * 2 + b) * 2 + c,
            )
            copy.start()
            sends.append(copy)
    for i in range(1, planes):
        ref = z_in.at[i]
        remote(ref, ref, z_sem.at[1, i], z_sem.at[1, i], me).wait_recv()
        total = total + z_in[i].astype(F32)
    mixed_ref[...] = total.astype(BF16)
    gather.drain()
    for copy in sends:
        copy.wait_send()


VM = pl.BlockSpec(memory_space=pltpu.VMEM)
ANY = pl.BlockSpec(memory_space=pl.ANY)
HBM = pl.BlockSpec(memory_space=pltpu.HBM)


def cost(us):
    return pl.CostEstimate(flops=int(us * 2e7), bytes_accessed=2**20, transcendentals=0)


def shards(
    hidden_in, state_in, norm_gain, w_recept, w_key, w_value, decay_base, w_decay_down,
    w_decay_up, w_remove_down, w_remove_up, group_gain, w_out, ffn_gain, routes, route_gate,
    w_gate, w_up, w_down,
):
    ep_size = lax.axis_size("ep")
    experts = ep_size // EXP_SPLIT
    rows, width = hidden_in.shape
    head, inner = state_in.shape[1:]
    part = w_recept.shape[1]
    lanes = -(-(3 * part + 2 * experts) // 128) * 128
    half, planes = ep_size // 2, ep_size // 4

    def like(array):
        return pltpu.VMEM(array.shape, array.dtype)

    loaded = (w_decay_down, w_decay_up, w_remove_down, w_remove_up)
    w_gate, w_up = w_gate.T, w_up.T
    got, decay, removal = pl.pallas_call(
        functools.partial(project_kernel, ep_size, experts),
        out_shape=(
            jax.ShapeDtypeStruct((2, half, rows, lanes), BF16),
            jax.ShapeDtypeStruct((rows, inner), F32),
            jax.ShapeDtypeStruct((rows, inner), F32),
        ),
        in_specs=[VM] * 5 + [HBM] * 7,
        out_specs=(VM, VM, VM),
        scratch_shapes=[like(w) for w in loaded]
        + [pltpu.SemaphoreType.DMA((7,)), pltpu.VMEM((lanes, width), BF16)]
        + gather_scratch(ep_size, rows, width)
        + [
            pltpu.VMEM((2, half, rows, lanes), BF16),
            pltpu.VMEM((2, half, rows, lanes), BF16),
            pltpu.SemaphoreType.DMA((ep_size,)),
            pltpu.SemaphoreType.DMA((ep_size,)),
        ],
        compiler_params=pltpu.CompilerParams(
            collective_id=0, has_side_effects=True, vmem_limit_bytes=20 * 2**20
        ),
        cost_estimate=cost(20000),
        name="project",
    )(
        hidden_in, norm_gain.reshape(1, -1), decay_base.reshape(1, -1), routes, route_gate,
        w_recept.T, w_key.T, w_value.T, *loaded
    )

    seqs = min(8, rows)
    whole = lambda *shape: pl.BlockSpec(shape, lambda s: (0,) * len(shape))
    state_spec = pl.BlockSpec((seqs, head, inner), lambda s: (s, 0, 0))
    state_out, residual, expert_in = pl.pallas_call(
        functools.partial(mixer_kernel, ep_size),
        grid=(rows // seqs,),
        out_shape=(
            jax.ShapeDtypeStruct(state_in.shape, F32),
            jax.ShapeDtypeStruct((rows, width), F32),
            jax.ShapeDtypeStruct((rows, width), BF16),
        ),
        in_specs=[
            whole(rows, width),
            whole(2, half, rows, lanes),
            whole(rows, inner),
            whole(rows, inner),
            whole(1, inner),
            whole(1, width),
            state_spec,
            ANY,
        ],
        out_specs=(state_spec, whole(rows, width), whole(rows, width)),
        scratch_shapes=[
            like(w_out),
            pltpu.SemaphoreType.DMA,
            pltpu.VMEM((rows, inner), F32),
            pltpu.VMEM((rows, inner), F32),
            pltpu.VMEM((rows, inner), F32),
            pltpu.VMEM((inner, inner // head), BF16),
            pltpu.VMEM((rows, inner), F32),
        ],
        compiler_params=pltpu.CompilerParams(
            dimension_semantics=("arbitrary",), vmem_limit_bytes=32 * 2**20
        ),
        cost_estimate=cost(10000),
        name="mixer",
    )(
        hidden_in, got, decay, removal, group_gain.reshape(1, -1), ffn_gain.reshape(1, -1),
        state_in, w_out,
    )

    mixed_out = pl.pallas_call(
        functools.partial(expert_kernel, ep_size, experts, part),
        out_shape=jax.ShapeDtypeStruct((rows, width), BF16),
        in_specs=[VM] * 3 + [ANY] * 3,
        out_specs=VM,
        scratch_shapes=[like(w_gate), like(w_up), like(w_down), pltpu.SemaphoreType.DMA((3,))]
        + gather_scratch(ep_size, rows, width)
        + [
            pltpu.VMEM((half, rows, width), F32),
            pltpu.VMEM((half, rows, width), BF16),
            pltpu.VMEM((half, rows, width), BF16),
            pltpu.SemaphoreType.DMA((2, planes)),
            pltpu.VMEM((planes, rows, width), BF16),
            pltpu.VMEM((planes, rows, width), BF16),
            pltpu.SemaphoreType.DMA((2, planes)),
            pltpu.VMEM((planes, rows, width), BF16),
            pltpu.VMEM((planes, rows, width), BF16),
            pltpu.SemaphoreType.DMA((2, planes)),
        ],
        compiler_params=pltpu.CompilerParams(
            collective_id=1, has_side_effects=True, vmem_limit_bytes=48 * 2**20
        ),
        cost_estimate=cost(20000),
        name="experts",
    )(expert_in, residual, got, w_gate, w_up, w_down)
    return (mixed_out, state_out)


def solution(mesh):
    placed = (
        P(("grp", "ep"), None),
        P(("grp", "ep"), None, None),
        P(),
        P(None, "ep"),
        P(None, "ep"),
        P(None, "ep"),
        P(),
        P(),
        P(),
        P(),
        P(),
        P(),
        P(),
        P(),
        P(("grp", "ep"), None),
        P(("grp", "ep"), None),
        P(None, "ep"),
        P(None, "ep"),
        P("ep", None),
    )
    return jax.shard_map(
        shards,
        mesh=mesh,
        in_specs=placed,
        out_specs=(P(("grp", "ep"), None), P(("grp", "ep"), None, None)),
        check_vma=False,
    )
```

time: 199 us -> 86.4 us (0.43)
  Pallas kernels: 0 us -> 73.9 us
  waiting for transfers between devices: 38.7 us -> 0 us
  local copies, waits for them, and re-layouts: 47.2 us -> 11.2 us
  blocking collectives: 30.5 us -> 0 us
  matrix products: 30.2 us -> 0 us
  other arithmetic: 28 us -> 0 us
  between operations: 14.4 us -> 0.75 us
  starting transfers between devices: 8.8 us -> 0 us
    pallas_call x0 -> x3, Pallas kernels: none -> 73.9 us  [the longest x1 33.4 us: shards(): pl.pallas_call(functools.partial(expert_kernel, ep_size, experts, part),...]
    all_gather x1 -> x0, waiting for transfers between devices: 38.6 us -> none  [shards(): shard_rows = lax.all_gather(normed, 'ep', axis=0, tiled=True)]
    all_to_all x1 -> x0, blocking collectives: 30.5 us -> none  [shards(): lax.all_to_all(send_buffer, 'ep', split_axis=0, concat_axis=0, tiled=True)]
    dot_general x11 -> x0, matrix products: 30.2 us -> none  [the longest x1 8.51 us: update_state(): jnp.einsum('svhk,shk->shv', updated, recept_heads, precision=lax.Precisio...]
    mul x9 -> x0, local copies, waits for them, and re-layouts: 28.3 us -> none  [the longest x2 13.5 us: update_state(): recalled[..., None] * removed[:, None]]
    add x2 -> x0, other arithmetic: 14 us -> none  [update_state(): blocks * decay_rate.reshape(seq_count, 1, head_count, head_size)]
    reshape x3 -> x0, local copies, waits for them, and re-layouts: 10.5 us -> none  [the longest x1 7.28 us: update_state(): blocks = state_in.reshape(seq_count, head_size, head_count, head_size)]
    all_to_all x2 -> x0, starting transfers between devices: 8.76 us -> none  [the longest x1 5.07 us: shards(): lax.all_to_all(partial_out, 'ep', split_axis=0, concat_axis=0, tiled=True)]
  transfers between devices with their start and end apart: 3 -> 0, of which waited for: 1 -> 0; matrix products, arithmetic and copies ran while one was open for 23% -> 0% of each run, Pallas kernels for 0% -> 0%
where the time goes in v1:
time: 86.4 us; the launch traced here: 85.9 us
  Pallas kernels  73.9 us (86%)
  local copies, waits for them, and re-layouts  11.2 us (13%)
    pallas_call x1, Pallas kernels, shards(): pl.pallas_call(functools.partial(expert_kernel, ep_size, experts, part),...  33.4 us
    pallas_call x1, Pallas kernels, shards(): pl.pallas_call(functools.partial(project_kernel, ep_size, experts), out_s...  25.2 us
    pallas_call x1, Pallas kernels, shards(): pl.pallas_call(functools.partial(mixer_kernel, ep_size), grid=(rows // se...  15.4 us
    unnamed x37, local copies, waits for them, and re-layouts  11.2 us

profile of v1, /device:TPU:0, one launch (start us, length us, event | category | flops | bytes accessed | tf_op | source)
XLA Modules:
  0.0 85.9 jit_solution(3795773477325265619)
XLA Ops:
  0.6 0.8 copy.21.routes_ref
  1.4 0.8 copy.22.gates_ref
  2.1 0.0 copy-start.4
  2.1 1.0 %copy-done.4 = bf16[2048,128]{1,0:T(8,128)(2,1)S(1)} copy-done((bf16[2048,128]{1,0:T(8,128)(2,1)S(1)}, bf16[2048,128]{1,0:T(8,128)(2,1)}, u32[]{:S(2)}) %copy-start.4) | copy-done | bytes 524312
  3.2 0.0 copy-start.5
  3.2 1.0 %copy-done.5 = bf16[2048,128]{1,0:T(8,128)(2,1)S(1)} copy-done((bf16[2048,128]{1,0:T(8,128)(2,1)S(1)}, bf16[2048,128]{1,0:T(8,128)(2,1)}, u32[]{:S(2)}) %copy-start.5) | copy-done | bytes 524312
  4.2 0.0 copy-start.6
  4.2 0.9 %copy-done.6 = bf16[2048,64]{0,1:T(8,128)(2,1)S(1)} copy-done((bf16[2048,64]{0,1:T(8,128)(2,1)S(1)}, bf16[2048,64]{0,1:T(8,128)(2,1)}, u32[]{:S(2)}) %copy-start.6) | copy-done | bytes 262168
  5.2 0.0 copy-start.7
  5.2 0.9 %copy-done.7 = bf16[2048,64]{0,1:T(8,128)(2,1)S(1)} copy-done((bf16[2048,64]{0,1:T(8,128)(2,1)S(1)}, bf16[2048,64]{0,1:T(8,128)(2,1)}, u32[]{:S(2)}) %copy-start.7) | copy-done | bytes 262168
  6.1 0.0 copy-start.8
  6.1 0.9 %copy-done.8 = bf16[2048,64]{0,1:T(8,128)(2,1)S(1)} copy-done((bf16[2048,64]{0,1:T(8,128)(2,1)S(1)}, bf16[2048,64]{0,1:T(8,128)(2,1)}, u32[]{:S(2)}) %copy-start.8) | copy-done | bytes 262168
  7.1 0.0 copy-start.9
  7.1 0.9 %copy-done.9 = bf16[128,1024]{1,0:T(8,128)(2,1)S(1)} copy-done((bf16[128,1024]{1,0:T(8,128)(2,1)S(1)}, bf16[128,1024]{1,0:T(8,128)(2,1)}, u32[]{:S(2)}) %copy-start.9) | copy-done | bytes 262168
  8.0 0.0 copy-start.10
  8.0 0.9 %copy-done.10 = bf16[128,1024]{1,0:T(8,128)(2,1)S(1)} copy-done((bf16[128,1024]{1,0:T(8,128)(2,1)S(1)}, bf16[128,1024]{1,0:T(8,128)(2,1)}, u32[]{:S(2)}) %copy-start.10) | copy-done | bytes 262168
  9.0 0.0 copy-start.11
  9.0 0.8 copy-done.11
  9.8 0.0 copy-start.13
  9.8 0.7 copy-done.13
  10.5 0.0 copy-start.15
  10.5 0.7 copy-done.15
  11.2 0.0 copy-start
  11.2 0.0 copy-start.1
  11.2 0.0 copy-start.12
  11.2 0.0 copy-start.14
  11.2 0.0 copy-start.16
  11.2 25.2 %project.1 = (bf16[2,8,16,256]{3,2,1,0:T(8,128)(2,1)S(1)}, f32[16,1024]{1,0:T(8,128)S(1)}, f32[16,1024]{1,0:T(8,128)S(1)}) custom-call(bf16[16,2048]{1,0:T(8,128)(2,1)S(1)} %copy-done.11, f32[1,2048]{1,0:T(1,128)S(1)} %bitcast.14, f32[1,1024]{1,0:T(1,128)S(1)} %bitcast.16, s32[16,2]{1,0:T(8,128)S(1)} %copy.21.routes_ref, f32[16,2]{1,0:T(8,128)S(1)} %copy.22.gates_ref, ...), custom_call_target="tpu_custom_call" | custom-call | flops 399999991808 | bytes 1048576 | tf_op jit(solution)/shard_map/project/pallas_call | solution.py:419
  36.4 0.0 copy-done
  36.4 0.0 copy-done.1
  36.4 0.0 copy-done.12
  36.4 0.0 copy-done.14
  36.4 0.0 copy-done.16
  36.4 0.0 copy-start.2
  36.5 0.0 copy-start.3
  36.5 15.4 %mixer.1 = (f32[16,64,1024]{2,1,0:T(8,128)}, f32[16,2048]{1,0:T(8,128)S(1)}, bf16[16,2048]{1,0:T(8,128)(2,1)S(1)}) custom-call(bf16[16,2048]{1,0:T(8,128)(2,1)S(1)} %copy-done.12, bf16[2,8,16,256]{3,2,1,0:T(8,128)(2,1)S(1)} %get-tuple-element.8.got_ref, f32[16,1024]{1,0:T(8,128)S(1)} %get-tuple-element.9.decay_ref, ...), custom_call_target="tpu_custom_call" | custom-call | flops 199999995904 | bytes 1048576 | tf_op jit(solution)/shard_map/mixer/pallas_call | solution.py:450
  51.8 0.0 copy-done.2
  51.9 0.0 copy-done.3
  51.9 33.4 %experts.1 = bf16[16,2048]{1,0:T(8,128)(2,1)S(1)} custom-call(bf16[16,2048]{1,0:T(8,128)(2,1)S(1)} %get-tuple-element.11.expert_ref, f32[16,2048]{1,0:T(8,128)S(1)} %get-tuple-element.12.residual_ref, bf16[2,8,16,256]{3,2,1,0:T(8,128)(2,1)S(1)} %get-tuple-element.8.got_ref, bf16[704,2048]{1,0:T(8,128)(2,1)S(1)} %bitcast.9, bf16[704,2048]{1,0:T(8,128)(2,1)S(1)} %bitcast.10, ...), custom_call_target="tpu_custom_call" | custom-call | flops 399999991808 | bytes 1048576 | tf_op jit(solution)/shard_map/experts/pallas_call | solution.py:488
  85.3 0.6 copy.24
Async XLA Ops:
  2.1 1.0 %copy-start.4 = (bf16[2048,128]{1,0:T(8,128)(2,1)S(1)}, bf16[2048,128]{1,0:T(8,128)(2,1)}, u32[]{:S(2)}) copy-start(bf16[2048,128]{1,0:T(8,128)(2,1)} %wdd.1) | copy-start | bytes 1572868
  3.2 1.0 %copy-start.5 = (bf16[2048,128]{1,0:T(8,128)(2,1)S(1)}, bf16[2048,128]{1,0:T(8,128)(2,1)}, u32[]{:S(2)}) copy-start(bf16[2048,128]{1,0:T(8,128)(2,1)} %wrd.1) | copy-start | bytes 1572868
  4.2 0.9 %copy-start.6 = (bf16[2048,64]{0,1:T(8,128)(2,1)S(1)}, bf16[2048,64]{0,1:T(8,128)(2,1)}, u32[]{:S(2)}) copy-start(bf16[2048,64]{0,1:T(8,128)(2,1)} %param.22) | copy-start | bytes 786436
  5.2 0.9 %copy-start.7 = (bf16[2048,64]{0,1:T(8,128)(2,1)S(1)}, bf16[2048,64]{0,1:T(8,128)(2,1)}, u32[]{:S(2)}) copy-start(bf16[2048,64]{0,1:T(8,128)(2,1)} %param.23) | copy-start | bytes 786436
  6.1 0.9 %copy-start.8 = (bf16[2048,64]{0,1:T(8,128)(2,1)S(1)}, bf16[2048,64]{0,1:T(8,128)(2,1)}, u32[]{:S(2)}) copy-start(bf16[2048,64]{0,1:T(8,128)(2,1)} %param.24) | copy-start | bytes 786436
  7.1 0.9 %copy-start.9 = (bf16[128,1024]{1,0:T(8,128)(2,1)S(1)}, bf16[128,1024]{1,0:T(8,128)(2,1)}, u32[]{:S(2)}) copy-start(bf16[128,1024]{1,0:T(8,128)(2,1)} %wdu.1) | copy-start | bytes 786436
  8.0 0.9 %copy-start.10 = (bf16[128,1024]{1,0:T(8,128)(2,1)S(1)}, bf16[128,1024]{1,0:T(8,128)(2,1)}, u32[]{:S(2)}) copy-start(bf16[128,1024]{1,0:T(8,128)(2,1)} %wru.1) | copy-start | bytes 786436
  9.0 0.8 copy-start.11
  9.8 0.7 copy-start.13
  10.5 0.7 copy-start.15
  11.2 25.2 %copy-start = (f32[16,64,1024]{2,1,0:T(8,128)S(1)}, f32[16,64,1024]{2,1,0:T(8,128)}, u32[]{:S(2)}) copy-start(f32[16,64,1024]{2,1,0:T(8,128)} %state_ref.1) | copy-start | bytes 12582916
  11.2 25.2 %copy-start.1 = (bf16[1024,2048]{1,0:T(8,128)(2,1)S(1)}, bf16[1024,2048]{1,0:T(8,128)(2,1)}, u32[]{:S(2)}) copy-start(bf16[1024,2048]{1,0:T(8,128)(2,1)} %w_out.1) | copy-start | bytes 12582916
  11.2 25.2 %copy-start.12 = (bf16[16,2048]{1,0:T(8,128)(2,1)S(1)}, bf16[16,2048]{1,0:T(8,128)(2,1)}, u32[]{:S(2)}) copy-start(bf16[16,2048]{1,0:T(8,128)(2,1)} %hidden_ref.3) | copy-start | bytes 196612
  11.2 25.2 %copy-start.14 = (f32[2048]{0:T(1024)S(1)}, f32[2048]{0:T(1024)}, u32[]{:S(2)}) copy-start(f32[2048]{0:T(1024)} %param.32) | copy-start | bytes 24580
  11.2 25.2 %copy-start.16 = (f32[1024]{0:T(1024)S(1)}, f32[1024]{0:T(1024)}, u32[]{:S(2)}) copy-start(f32[1024]{0:T(1024)} %param.30) | copy-start | bytes 12292
  36.4 15.4 %copy-start.2 = (bf16[2048,704]{0,1:T(8,128)(2,1)S(1)}, bf16[2048,704]{0,1:T(8,128)(2,1)}, u32[]{:S(2)}) copy-start(bf16[2048,704]{0,1:T(8,128)(2,1)} %param.35) | copy-start | bytes 8650756
  36.5 15.4 %copy-start.3 = (bf16[2048,704]{0,1:T(8,128)(2,1)S(1)}, bf16[2048,704]{0,1:T(8,128)(2,1)}, u32[]{:S(2)}) copy-start(bf16[2048,704]{0,1:T(8,128)(2,1)} %param.36) | copy-start | bytes 8650756

commit v2 on v1

--- a/solution.py
+++ b/solution.py
@@ -8,6 +8,8 @@
 from jax.sharding import PartitionSpec as P
 
 EXP_SPLIT = 4
+MIX = 4
+FULL = 67_043_328
 MESH = pl.DeviceIdType.MESH
 F32 = jnp.float32
 BF16 = jnp.bfloat16
@@ -73,7 +75,7 @@
 
     def slot(self, core, back, side):
         plane = lax.rem(self.a + (self.planes - back), self.planes)
-        return self.slots.at[core, plane * 2 + side]
+        return self.slots.at[plane, side, core]
 
     def device(self, plane, side, core):
         return (plane * 2 + side) * 2 + core
@@ -106,7 +108,7 @@
         self.sent.append(copy)
 
     def start(self):
-        for i in reversed(range(1, self.planes)):
+        for i in range(1, self.planes):
             self.go(self.along(i))
         self.go(self.across(0))
         self.go(self.to_core(0, 0))
@@ -118,18 +120,14 @@
         self.arrived(self.slot(self.c, i, 1 - self.b), self.bs.at[1, i])
         self.go(self.to_core(1, i))
 
-    def finish(self):
-        for i in range(1, self.planes):
-            self.arrived(self.slot(self.c, i, self.b), self.z.at[1, i])
-            self.go(self.across(i))
-            self.go(self.to_core(0, i))
-            self.relay_side(i - 1)
-        self.relay_side(self.planes - 1)
-
-    def finish_core(self):
-        for i in range(self.planes):
-            self.arrived(self.slot(1 - self.c, i, self.b), self.cs.at[1, 0, i])
-            self.arrived(self.slot(1 - self.c, i, 1 - self.b), self.cs.at[1, 1, i])
+    def relay_plane(self, i):
+        self.arrived(self.slot(self.c, i, self.b), self.z.at[1, i])
+        self.go(self.across(i))
+        self.go(self.to_core(0, i))
+
+    def whole_plane(self, i):
+        self.arrived(self.slot(1 - self.c, i, self.b), self.cs.at[1, 0, i])
+        self.arrived(self.slot(1 - self.c, i, 1 - self.b), self.cs.at[1, 1, i])
 
     def drain(self):
         for copy in self.sent:
@@ -139,7 +137,7 @@
 def gather_scratch(ep_size, rows, width):
     planes = ep_size // 4
     return [
-        pltpu.VMEM((2, ep_size // 2, rows, width), BF16),
+        pltpu.VMEM((planes, 2, 2, rows, width), BF16),
         pltpu.SemaphoreType.DMA((2, planes)),
         pltpu.SemaphoreType.DMA((2, planes)),
         pltpu.SemaphoreType.DMA((2, 2, planes)),
@@ -173,7 +171,7 @@
     if lanes > 3 * part:
         joint[3 * part :, :] = jnp.zeros((lanes - 3 * part, joint.shape[1]), BF16)
     normed = scaled_rows(hidden_ref[...], gain_ref[...]).astype(BF16)
-    slots[c, a * 2 + b] = normed
+    slots[a, b, c] = normed
     pl.semaphore_wait(barrier, ep_size - 1)
     gather = Gather(ep_size, slots, z_sems, b_sems, c_sems)
     gather.start()
@@ -188,37 +186,45 @@
     removal_ref[...] = jax.nn.sigmoid(dot(remove_low, wru_v[...]))
     for copy in loads[4:]:
         copy.wait()
-    lane = lax.broadcasted_iota(jnp.int32, (rows, lanes), 1) - 3 * part
-    weight = jnp.zeros((rows, lanes), F32)
-    for j in range(routes_ref.shape[1]):
-        chosen = routes_ref[:, j : j + 1]
+    lane = lax.broadcasted_iota(jnp.int32, (lanes, rows), 0) - 3 * part
+    weight = jnp.zeros((lanes, rows), F32)
+    for j in range(routes_ref.shape[0]):
+        chosen = routes_ref[j : j + 1, :]
         hit = (lane == chosen) | (lane == chosen + experts)
-        weight = weight + jnp.where(hit, gates_ref[:, j : j + 1], 0.0)
+        weight = weight + jnp.where(hit, gates_ref[j : j + 1, :], 0.0)
     high = weight.astype(BF16).astype(F32)
     spare = jnp.where(lane < experts, high, weight - high)
-    spare = jnp.where(lane >= 0, spare, 0.0)
-
-    gather.finish()
-    gather.finish_core()
+    spare = jnp.where(lane >= 0, spare, 0.0).astype(BF16)
+    same = lax.broadcasted_iota(jnp.int32, (rows, rows), 0) == lax.broadcasted_iota(
+        jnp.int32, (rows, rows), 1
+    )
+    spare = dot_t(same.astype(F32).astype(BF16), spare)
+
+    for i in range(1, planes):
+        gather.relay_plane(i)
+        gather.relay_side(i - 1)
+    gather.relay_side(planes - 1)
+    for i in range(planes):
+        gather.whole_plane(i)
     rows_all = slots[...].reshape(ep_size * rows, width)
-    spread = dot_t(rows_all, joint[...]).reshape(2, ep_size // 2, rows, lanes)
-    outbox[...] = (spread + spare[None, None]).astype(BF16)
+    spread = dot_t(rows_all, joint[...]).reshape(ep_size, rows, lanes)
+    outbox[...] = (spread + spare[None]).astype(BF16)
     sends = []
     for step in range(1, ep_size):
         other = lax.rem(me + step, ep_size)
         copy = remote(
-            outbox.at[other % 2, other // 2],
-            inbox.at[c, a * 2 + b],
+            outbox.at[other],
+            inbox.at[me],
             x_send.at[step],
             x_recv.at[step],
             other,
         )
         copy.start()
         sends.append(copy)
-    inbox[c, a * 2 + b] = outbox[c, a * 2 + b]
+    inbox[me] = outbox[me]
     for step in range(1, ep_size):
         other = lax.rem(me + (ep_size - step), ep_size)
-        ref = inbox.at[other % 2, other // 2]
+        ref = inbox.at[other]
         remote(ref, ref, x_recv.at[step], x_recv.at[step], me).wait_recv()
     got_ref[...] = inbox[...]
     gather.drain()
@@ -241,7 +247,7 @@
     def _():
         load.start()
         for d in range(ep_size):
-            block = got_ref[d % 2, d // 2].astype(F32)
+            block = got_ref[d].astype(F32)
             own = slice(d * part, (d + 1) * part)
             recept[:, own] = block[:, 0:part]
             keys[:, own] = block[:, part : 2 * part]
@@ -269,22 +275,33 @@
     value_now = values[these, :]
     decay = decay_ref[these, :]
     out_rows = []
-    for s in range(seqs):
-        one = slice(s, s + 1)
-        block = state_ref[s]
-        recalled = split_dot(block * unit[one], gather)
-        value_col = dot((own_row * value_now[one]).astype(BF16), gather)
+    for first in range(0, seqs, MIX):
+        ones = [slice(n, n + 1) for n in range(first, first + MIX)]
+
+        def by_row(table):
+            return jnp.concatenate(
+                [jnp.broadcast_to(table[one], (head, inner)) for one in ones], axis=0
+            )
+
+        block = state_ref[first : first + MIX].reshape(MIX * head, inner)
+        recalled = dot((block * by_row(unit)).astype(BF16), gather)
+        diagonal = jnp.concatenate([own_row * value_now[one] for one in ones], axis=0)
+        value_col = dot(diagonal.astype(BF16), gather)
         updated = (
-            block * decay[one]
-            - split_dot(recalled, spread) * removed[one]
-            + dot(value_col.astype(BF16), spread) * key[one]
+            block * by_row(decay)
+            - dot(recalled.astype(BF16), spread) * by_row(removed)
+            + dot(value_col.astype(BF16), spread) * by_row(key)
         )
-        state_out[s] = updated
-        readout = split_dot(updated * recept_now[one], gather)
-        center = readout - jnp.mean(readout, axis=0, keepdims=True)
-        var = jnp.mean(center * center, axis=0, keepdims=True)
-        normed = center * lax.rsqrt(var + group_eps)
-        out_rows.append(jnp.sum(split_dot(normed, spread) * own_row, axis=0, keepdims=True))
+        state_out[first : first + MIX] = updated.reshape(MIX, head, inner)
+        readout = dot((updated * by_row(recept_now)).astype(BF16), gather)
+        readout = readout.reshape(MIX, head, heads)
+        center = readout - jnp.mean(readout, axis=1, keepdims=True)
+        var = jnp.mean(center * center, axis=1, keepdims=True)
+        normed = (center * lax.rsqrt(var + group_eps)).reshape(MIX * head, heads)
+        wide = dot(normed.astype(BF16), spread)
+        for n in range(MIX):
+            one = wide[n * head : (n + 1) * head] * own_row
+            out_rows.append(jnp.sum(one, axis=0, keepdims=True))
     grouped[these, :] = jnp.concatenate(out_rows, axis=0) * ggain_ref[...]
 
     @pl.when(step == pl.num_programs(0) - 1)
@@ -300,88 +317,108 @@
     mixed_ref,
     wg_v, wu_v, wd_v, load_sems,
     slots, z_sems, b_sems, c_sems,
-    mine, c_out, c_in, c_sem, b_out, b_in, b_sem, z_out, z_in, z_sem,
+    partial, c_out, c_in, c_sem, b_out, b_in, b_sem, z_out, z_in, z_sem,
 ):
     me, a, b, c, planes = place(ep_size)
     rows, width = expert_ref.shape
-    half = ep_size // 2
+    half = planes // 2
     barrier = greet_all(me, ep_size)
     loads = load_all([(wg, wg_v), (wu, wu_v), (wd, wd_v)], load_sems)
-    slots[c, a * 2 + b] = expert_ref[...]
+    slots[a, b, c] = expert_ref[...]
     pl.semaphore_wait(barrier, ep_size - 1)
     gather = Gather(ep_size, slots, z_sems, b_sems, c_sems)
     gather.start()
     expert = me // EXP_SPLIT
-    lane = lax.broadcasted_iota(jnp.int32, got_ref.shape[2:], 1) - 3 * part
+    lane = lax.broadcasted_iota(jnp.int32, got_ref.shape[1:], 1) - 3 * part
     column = (lane == expert) | (lane == expert + experts)
+    sends = []
+
+    def back(i):
+        return lax.rem(a + (planes - i), planes)
+
+    def send(src, dst, sems, i, device):
+        copy = remote(src.at[i], dst.at[i], sems.at[0, i], sems.at[1, i], device)
+        copy.start()
+        sends.append(copy)
+
+    def landed(dst, sems, i):
+        remote(dst.at[i], dst.at[i], sems.at[1, i], sems.at[1, i], me).wait_recv()
+
+    def run(span, after_gate, after_up):
+        flat = jnp.concatenate([slots[back(i)].reshape(4 * rows, width) for i in span], axis=0)
+        gate_pre = dot_t(flat, wg_v[...])
+        after_gate()
+        up_pre = dot_t(flat, wu_v[...])
+        after_up()
+        hidden = (jax.nn.silu(gate_pre) * up_pre).astype(BF16)
+        down = dot(hidden, wd_v[...])
+        for n, i in enumerate(span):
+            weight = jnp.concatenate(
+                [
+                    jnp.sum(
+                        jnp.where(column, got_ref[back(i) * 4 + m].astype(F32), 0.0),
+                        axis=-1,
+                        keepdims=True,
+                    )
+                    for m in range(4)
+                ],
+                axis=0,
+            )
+            own = down[n * 4 * rows : (n + 1) * 4 * rows] * weight
+            partial[i] = own.reshape(2, 2, rows, width)
+
+    def send_core(i):
+        c_out[i] = partial[i, :, 1 - c].astype(BF16)
+        send(c_out, c_in, c_sem, i, (a * 2 + b) * 2 + 1 - c)
+
+    def send_side(i):
+        landed(c_in, c_sem, i)
+        b_out[i] = (partial[i, 1 - b, c] + c_in[i, 1 - b].astype(F32)).astype(BF16)
+        send(b_out, b_in, b_sem, i, (a * 2 + 1 - b) * 2 + c)
+
+    def joined(i):
+        landed(b_in, b_sem, i)
+        return partial[i, b, c] + c_in[i, b].astype(F32) + b_in[i].astype(F32)
+
+    def send_plane(i):
+        z_out[i] = joined(i).astype(BF16)
+        send(z_out, z_in, z_sem, i, (back(i) * 2 + b) * 2 + c)
+
+    first, second = list(range(half)), list(range(half, planes))
+    for i in first[1:]:
+        gather.relay_plane(i)
+    for i in first:
+        gather.relay_side(i)
+    for i in first:
+        gather.whole_plane(i)
     for copy in loads:
         copy.wait()
 
-    def run(core):
-        flat = slots[core].reshape(half * rows, width)
-        gate_pre = dot_t(flat, wg_v[...])
-        up_pre = dot_t(flat, wu_v[...])
-        hidden = (jax.nn.silu(gate_pre) * up_pre).astype(BF16)
-        weight = jnp.sum(
-            jnp.where(column[None], got_ref[core].astype(F32), 0.0), axis=-1, keepdims=True
-        )
-        return dot(hidden, wd_v[...]).reshape(half, rows, width) * weight
-
-    gather.finish()
-    gather.finish_core()
-    sends = []
-    c_out[...] = run(1 - c).astype(BF16)
-    for i in range(planes):
-        plane = lax.rem(a + i, planes)
-        copy = remote(
-            c_out.at[pl.ds(plane * 2, 2)],
-            c_in.at[pl.ds(plane * 2, 2)],
-            c_sem.at[0, i],
-            c_sem.at[1, i],
-            (a * 2 + b) * 2 + 1 - c,
-        )
-        copy.start()
-        sends.append(copy)
-    mine[...] = run(c)
-    order = list(range(1, planes)) + [0]
-    for i in order:
-        plane = lax.rem(a + i, planes)
-        both = c_in.at[pl.ds(plane * 2, 2)]
-        remote(both, both, c_sem.at[1, i], c_sem.at[1, i], me).wait_recv()
-        far = plane * 2 + 1 - b
-        b_out[plane] = (mine[far] + c_in[far].astype(F32)).astype(BF16)
-        copy = remote(
-            b_out.at[plane],
-            b_in.at[plane],
-            b_sem.at[0, i],
-            b_sem.at[1, i],
-            (a * 2 + 1 - b) * 2 + c,
-        )
-        copy.start()
-        sends.append(copy)
-    total = residual_ref[...]
-    for i in order:
-        plane = lax.rem(a + i, planes)
-        ref = b_in.at[plane]
-        remote(ref, ref, b_sem.at[1, i], b_sem.at[1, i], me).wait_recv()
-        near = plane * 2 + b
-        joined = mine[near] + c_in[near].astype(F32) + b_in[plane].astype(F32)
-        if i == 0:
-            total = total + joined
-        else:
-            z_out[i] = joined.astype(BF16)
-            copy = remote(
-                z_out.at[i],
-                z_in.at[i],
-                z_sem.at[0, i],
-                z_sem.at[1, i],
-                (plane * 2 + b) * 2 + c,
-            )
-            copy.start()
-            sends.append(copy)
+    def relay(span):
+        for i in span:
+            gather.relay_plane(i)
+
+    run(first, lambda: relay(second[:1]), lambda: None)
+    for i in reversed(first):
+        send_core(i)
+    relay(second[1:])
+    for i in second[:-1]:
+        gather.relay_side(i)
+    for i in reversed(first):
+        send_side(i)
+    gather.relay_side(second[-1])
+    for i in second:
+        gather.whole_plane(i)
+    run(second, lambda: None, lambda: [send_plane(i) for i in first[1:]])
+    for i in second:
+        send_core(i)
+    for i in second:
+        send_side(i)
+    for i in second:
+        send_plane(i)
+    total = residual_ref[...] + joined(0)
     for i in range(1, planes):
-        ref = z_in.at[i]
-        remote(ref, ref, z_sem.at[1, i], z_sem.at[1, i], me).wait_recv()
+        landed(z_in, z_sem, i)
         total = total + z_in[i].astype(F32)
     mixed_ref[...] = total.astype(BF16)
     gather.drain()
@@ -409,7 +446,7 @@
     head, inner = state_in.shape[1:]
     part = w_recept.shape[1]
     lanes = -(-(3 * part + 2 * experts) // 128) * 128
-    half, planes = ep_size // 2, ep_size // 4
+    planes = ep_size // 4
 
     def like(array):
         return pltpu.VMEM(array.shape, array.dtype)
@@ -419,7 +456,7 @@
     got, decay, removal = pl.pallas_call(
         functools.partial(project_kernel, ep_size, experts),
         out_shape=(
-            jax.ShapeDtypeStruct((2, half, rows, lanes), BF16),
+            jax.ShapeDtypeStruct((ep_size, rows, lanes), BF16),
             jax.ShapeDtypeStruct((rows, inner), F32),
             jax.ShapeDtypeStruct((rows, inner), F32),
         ),
@@ -429,18 +466,18 @@
         + [pltpu.SemaphoreType.DMA((7,)), pltpu.VMEM((lanes, width), BF16)]
         + gather_scratch(ep_size, rows, width)
         + [
-            pltpu.VMEM((2, half, rows, lanes), BF16),
-            pltpu.VMEM((2, half, rows, lanes), BF16),
+            pltpu.VMEM((ep_size, rows, lanes), BF16),
+            pltpu.VMEM((ep_size, rows, lanes), BF16),
             pltpu.SemaphoreType.DMA((ep_size,)),
             pltpu.SemaphoreType.DMA((ep_size,)),
         ],
         compiler_params=pltpu.CompilerParams(
-            collective_id=0, has_side_effects=True, vmem_limit_bytes=20 * 2**20
+            collective_id=0, has_side_effects=True, vmem_limit_bytes=FULL
         ),
         cost_estimate=cost(20000),
         name="project",
     )(
-        hidden_in, norm_gain.reshape(1, -1), decay_base.reshape(1, -1), routes, route_gate,
+        hidden_in, norm_gain.reshape(1, -1), decay_base.reshape(1, -1), routes.T, route_gate.T,
         w_recept.T, w_key.T, w_value.T, *loaded
     )
 
@@ -457,7 +494,7 @@
         ),
         in_specs=[
             whole(rows, width),
-            whole(2, half, rows, lanes),
+            whole(ep_size, rows, lanes),
             whole(rows, inner),
             whole(rows, inner),
             whole(1, inner),
@@ -476,7 +513,7 @@
             pltpu.VMEM((rows, inner), F32),
         ],
         compiler_params=pltpu.CompilerParams(
-            dimension_semantics=("arbitrary",), vmem_limit_bytes=32 * 2**20
+            dimension_semantics=("arbitrary",), vmem_limit_bytes=FULL
         ),
         cost_estimate=cost(10000),
         name="mixer",
@@ -493,9 +530,9 @@
         scratch_shapes=[like(w_gate), like(w_up), like(w_down), pltpu.SemaphoreType.DMA((3,))]
         + gather_scratch(ep_size, rows, width)
         + [
-            pltpu.VMEM((half, rows, width), F32),
-            pltpu.VMEM((half, rows, width), BF16),
-            pltpu.VMEM((half, rows, width), BF16),
+            pltpu.VMEM((planes, 2, 2, rows, width), F32),
+            pltpu.VMEM((planes, 2, rows, width), BF16),
+            pltpu.VMEM((planes, 2, rows, width), BF16),
             pltpu.SemaphoreType.DMA((2, planes)),
             pltpu.VMEM((planes, rows, width), BF16),
             pltpu.VMEM((planes, rows, width), BF16),
@@ -505,7 +542,7 @@
             pltpu.SemaphoreType.DMA((2, planes)),
         ],
         compiler_params=pltpu.CompilerParams(
-            collective_id=1, has_side_effects=True, vmem_limit_bytes=48 * 2**20
+            collective_id=1, has_side_effects=True, vmem_limit_bytes=FULL
         ),
         cost_estimate=cost(20000),
         name="experts",

time: 86.4 us -> 69.4 us (0.80)
  local copies, waits for them, and re-layouts: 11.2 us -> 1.47 us
  Pallas kernels: 73.9 us -> 67 us
    unnamed x37 -> x1, local copies, waits for them, and re-layouts: 11.2 us -> 1.47 us
    pallas_call x1, Pallas kernels: 15.4 us -> 9.32 us  [shards(): pl.pallas_call(functools.partial(mixer_kernel, ep_size), grid=(rows // se...]
where the time goes in v2:
time: 69.4 us; the launch traced here: 69.2 us
  Pallas kernels  67 us (97%)
  local copies, waits for them, and re-layouts  1.47 us (2%)
    pallas_call x1, Pallas kernels, shards(): pl.pallas_call(functools.partial(expert_kernel, ep_size, experts, part),...  32.7 us
    pallas_call x1, Pallas kernels, shards(): pl.pallas_call(functools.partial(project_kernel, ep_size, experts), out_s...  25 us
    pallas_call x1, Pallas kernels, shards(): pl.pallas_call(functools.partial(mixer_kernel, ep_size), grid=(rows // se...  9.32 us
    unnamed x1, local copies, waits for them, and re-layouts  1.47 us

profile of v2, /device:TPU:0, one launch (start us, length us, event | category | flops | bytes accessed | tf_op | source)
XLA Modules:
  0.0 69.2 jit_solution(7217916661712108862)
XLA Ops:
  0.6 25.0 %project.1 = (bf16[16,16,256]{2,1,0:T(8,128)(2,1)}, f32[16,1024]{1,0:T(8,128)}, f32[16,1024]{1,0:T(8,128)}) custom-call(bf16[16,2048]{1,0:T(8,128)(2,1)} %hidden_ref.3, f32[1,2048]{1,0:T(1,128)} %bitcast.16, f32[1,1024]{1,0:T(1,128)} %bitcast.18, s32[2,16]{1,0:T(2,128)} %bitcast.20, f32[2,16]{1,0:T(2,128)} %bitcast.21, bf16[64,2048]{1,0:T(8,128)(2,1)} %bitcast.13, ...), custom_call_target="tpu_custom_call" | custom-call | flops 399999991808 | bytes 1048576 | tf_op jit(solution)/shard_map/project/pallas_call | solution.py:456
  25.6 9.3 %mixer.1 = (f32[16,64,1024]{2,1,0:T(8,128)}, f32[16,2048]{1,0:T(8,128)}, bf16[16,2048]{1,0:T(8,128)(2,1)}) custom-call(bf16[16,2048]{1,0:T(8,128)(2,1)} %hidden_ref.3, bf16[16,16,256]{2,1,0:T(8,128)(2,1)} %get-tuple-element.8.got_ref, f32[16,1024]{1,0:T(8,128)} %get-tuple-element.9.decay_ref, f32[16,1024]{1,0:T(8,128)} %get-tuple-element.10.removal_ref, ...), custom_call_target="tpu_custom_call" | custom-call | flops 199999995904 | bytes 1048576 | tf_op jit(solution)/shard_map/mixer/pallas_call | solution.py:487
  35.0 32.7 %experts.1 = bf16[16,2048]{1,0:T(8,128)(2,1)} custom-call(bf16[16,2048]{1,0:T(8,128)(2,1)} %get-tuple-element.11.expert_ref, f32[16,2048]{1,0:T(8,128)} %get-tuple-element.12.residual_ref, bf16[16,16,256]{2,1,0:T(8,128)(2,1)} %get-tuple-element.8.got_ref, bf16[704,2048]{1,0:T(8,128)(2,1)} %bitcast.11, bf16[704,2048]{1,0:T(8,128)(2,1)} %bitcast.12, ...), custom_call_target="tpu_custom_call" | custom-call | flops 399999991808 | bytes 1048576 | tf_op jit(solution)/shard_map/experts/pallas_call | solution.py:525
  67.7 1.5 %copy.22 = bf16[16,2048]{1,0:T(8,128)(2,1)} copy(bf16[16,2048]{1,0:T(8,128)(2,1)} %experts.1) | data formatting | bytes 131072
